TPU v7x, 512 devices: a whole 4x8x8 slice. The times are simulated.
512 devices in a mesh: rep: 2 (over z_hi), fs: 32 (over z_lo, y), tp: 8 (over x, core).
Axes of the slice: x: 4, y: 8, z: 8 (z_hi: 2, z_lo: 4; z = z_hi * 4 + z_lo), core: 2. Of those that a mesh axis runs over, the one named last changes fastest.
Arguments:
- states: bfloat16 [24576, 2048], P(('rep', 'fs'), 'tp'), may hold values from -6 to 6
- mix_gain: float32 [2048], replicated, may hold values from 0.1 to 1.9
- w_value: bfloat16 [2048, 2048], P('fs', 'tp'), may hold values from -1 to 1
- w_gate: bfloat16 [2048, 2048], P('fs', 'tp'), may hold values from -0.125 to 0.125
- conv_kernel: float32 [31, 2048], replicated, may hold values from -1 to 1
- chan_gain: float32 [2048], replicated, may hold values from 0.1 to 1.9
- w_mix_out: bfloat16 [2048, 2048], P('fs', 'tp'), may hold values from -0.125 to 0.125
- mlp_gain: float32 [2048], replicated, may hold values from 0.1 to 1.9
- w_up: bfloat16 [2048, 6144], P('fs', 'tp'), may hold values from -0.125 to 0.125
- w_down_t: bfloat16 [2048, 6144], P('fs', 'tp'), may hold values from -0.078125 to 0.078125
Outputs:
- layer_out: bfloat16 [24576, 2048], P(('rep', 'fs'), 'tp')
All inputs are finite; a program needn't handle non-finite values.
Results may differ from a plain program's by a relative error of at most 0.017.
Values may be sent and summed in bfloat16 or wider, within the bound.
No kernel may reach another device: no remote copies, remote signals or barrier semaphores. Data moves between devices by JAX's collectives and lax.ppermute only.
A program may use at most 64 MiB of HBM per device.

v0:
```python
import jax
import jax.numpy as jnp
from jax import lax
from jax.sharding import Mesh
from jax.sharding import PartitionSpec as P

D = 2048
KWIDTH = 31
LENGTH = 128
TP = ("tp_0", "tp_1")


EPS = 1e-06


def cut_rows(length, count):
    hop = length // count
    if hop >= 8:
        hop -= hop % 8
    return [hop * k for k in range(1, count)]


def gather_in_order(shard, axes, order):
    pieces = shard
    for k in order:
        pieces = lax.all_gather(pieces, axes[k])
    done = order[::-1]
    back = [done.index(k) for k in range(len(axes))]
    pieces = pieces.transpose(*back, *range(len(axes), pieces.ndim))
    return pieces.reshape(-1, *shard.shape)


def laid_out(pieces, dim):
    pieces = jnp.moveaxis(pieces, 0, dim)
    dims = pieces.shape
    return pieces.reshape(*dims[:dim], dims[dim] * dims[dim + 1], *dims[dim + 2 :])


def gather_at_once(shard, axes, dim):
    split_at = max(range(max(1, shard.ndim - 1)), key=lambda d: shard.shape[d])
    count, outs = (len(axes), [])
    for initial, slab in enumerate(
        jnp.split(shard, cut_rows(shard.shape[split_at], count), axis=split_at)
    ):
        if slab.size:
            order = [(initial - k) % count for k in range(count)]
            outs.append(gather_in_order(slab, axes, order))
    return laid_out(jnp.concatenate(outs, axis=split_at + 1), dim)


def in_one_piece(arrays, axis, dim, along):
    ends, at = ([], 0)
    for a in arrays[:-1]:
        at += a.shape[along]
        ends.append(at)
    both = jnp.concatenate(arrays, axis=along)
    return tuple(jnp.split(lax.all_gather(both, axis, axis=dim, tiled=True), ends, axis=along))


def copy_for_each(shard, axis):
    copies = jnp.broadcast_to(shard, (lax.axis_size(axis), *shard.shape))
    return lax.all_to_all(copies, axis, split_axis=0, concat_axis=0, tiled=True)


def over_copies(shard, axis):
    everything = copy_for_each(shard, axis)
    return jnp.sum(everything, axis=0)


def in_one(arrays, axis):
    ends = [0]
    for a in arrays:
        ends.append(ends[-1] + a.size)
    so_far = over_copies(jnp.concatenate([a.ravel() for a in arrays]), axis)
    return tuple((so_far[b:e].reshape(a.shape) for a, b, e in zip(arrays, ends, ends[1:])))


def in_blocks(shard, dim, count):
    before, after = (shard.shape[:dim], shard.shape[dim + 1 :])
    return jnp.moveaxis(shard.reshape(*before, count, -1, *after), dim, 0)


def summed_on_arrival(shard, axis, dim):
    count = lax.axis_size(axis)
    pieces = lax.all_to_all(in_blocks(shard, dim, count), axis, 0, 0, tiled=True)
    return jnp.sum(pieces.astype(jnp.float32), axis=0)


def collect(shard, axis, dim):
    pieces = copy_for_each(shard, axis)
    return laid_out(pieces, dim)


def rms_norm(rows, gain):
    values = rows.astype(jnp.float32)
    scaled = values * lax.rsqrt(jnp.mean(values * values, axis=-1, keepdims=True) + EPS)
    return (scaled * gain).astype(jnp.bfloat16)


def times_transposed(left, right):
    return lax.dot_general(
        left, right, (((1,), (1,)), ((), ())), preferred_element_type=jnp.float32
    )


def body(
    states, mix_gain, w_value, w_gate, conv_kernel, chan_gain, w_mix_out, mlp_gain, w_up, w_down_t
):
    width = states.shape[1]
    offset = lax.axis_index(TP) * width
    token_rows = states.shape[0]
    whole_rows = gather_at_once(states, TP, 1)
    normed = rms_norm(whole_rows, mix_gain)
    value_full, gate_full, out_full = in_one_piece((w_value, w_gate, w_mix_out), "fs", 0, 1)
    value = jnp.dot(normed, value_full, preferred_element_type=jnp.float32)
    gate = jnp.dot(normed, gate_full, preferred_element_type=jnp.float32)
    gated = value * jax.nn.sigmoid(gate)
    own_kernel = lax.dynamic_slice_in_dim(conv_kernel, offset, width, 1)
    blocks = gated.reshape(token_rows // LENGTH, LENGTH, width)
    padded = jnp.pad(blocks, ((0, 0), (KWIDTH - 1, 0), (0, 0)))
    filtered = jnp.zeros_like(blocks)
    for tap in range(KWIDTH):
        filtered = filtered + own_kernel[tap][None, None, :] * padded[:, tap : tap + LENGTH, :]
    filtered = filtered.reshape(token_rows, width)
    sum_rows, square_rows = in_one(
        (jnp.sum(filtered, axis=-1), jnp.sum(filtered * filtered, axis=-1)), TP
    )
    mean_rows = (sum_rows / D)[:, None]
    variance = (square_rows / D)[:, None] - mean_rows * mean_rows
    own_gain = lax.dynamic_slice_in_dim(chan_gain, offset, width, 0)
    activated = jax.nn.silu((filtered - mean_rows) * lax.rsqrt(variance + EPS) * own_gain).astype(
        jnp.bfloat16
    )
    mixer_terms = times_transposed(activated, out_full)
    mixed = summed_on_arrival(mixer_terms.astype(jnp.bfloat16), TP, 1)
    middle = (states.astype(jnp.float32) + mixed).astype(jnp.bfloat16)
    middle_rows = collect(middle, TP, 1)
    normed_mid = rms_norm(middle_rows, mlp_gain)
    up_full, down_full = in_one_piece((w_up, w_down_t), "fs", 0, 1)
    upward = jnp.dot(normed_mid, up_full, preferred_element_type=jnp.float32)
    hidden = jnp.square(jnp.maximum(upward, 0.0)).astype(jnp.bfloat16)
    fed_terms = times_transposed(hidden, down_full)
    fed = summed_on_arrival(fed_terms.astype(jnp.bfloat16), TP, 1)
    return (middle.astype(jnp.float32) + fed).astype(jnp.bfloat16)


def solution(mesh):
    split = Mesh(
        mesh.devices.reshape(mesh.shape["rep"], mesh.shape["fs"], 4, 2),
        ("rep", "fs", "tp_0", "tp_1"),
    )
    return jax.shard_map(
        body,
        mesh=split,
        in_specs=(
            P(("rep", "fs"), TP),
            P(),
            P("fs", TP),
            P("fs", TP),
            P(),
            P(),
            P("fs", TP),
            P(),
            P("fs", TP),
            P("fs", TP),
        ),
        out_specs=P(("rep", "fs"), TP),
        check_vma=False,
    )
```

profile of v0, /device:TPU:1, one launch (start us, length us, event | category | flops | bytes accessed | tf_op | source)
XLA Modules:
  0.0 372.3 jit_solution(2018714799038196036)
XLA Ops:
  6.5 1.4 pad_maximum_fusion.2
  8.0 1.6 pad_maximum_fusion.1
  10.7 10.8 %all-gather = bf16[768,256]{1,0:T(8,128)(2,1)S(1)} all-gather(bf16[192,256]{1,0:T(8,128)(2,1)S(1)} %get-tuple-element.39), channel_id=2, replica_groups=mesh['rep'=2,'fs'=32,'tp_0'=4,'tp_1'=2] {'tp_0'}, dimensions={0}, use_global_device_ids=true | all-gather | bytes 491520 | tf_op jit(solution)/shard_map/all_gather | solution.py:26
  21.5 10.5 %all-gather.1 = bf16[8,192,256]{2,1,0:T(8,128)(2,1)S(1)} all-gather(bf16[4,192,256]{2,1,0:T(8,128)(2,1)S(1)} %bitcast.89), channel_id=3, replica_groups=mesh['rep'=2,'fs'=32,'tp_0'=4,'tp_1'=2] {'tp_1'}, dimensions={0}, use_global_device_ids=true | all-gather | bytes 1179648 | tf_op jit(solution)/shard_map/all_gather | solution.py:26
  32.1 2.0 all-gather.2
  34.0 11.8 %all-gather.3 = bf16[8,192,256]{2,1,0:T(8,128)(2,1)S(1)} all-gather(bf16[2,192,256]{2,1,0:T(8,128)(2,1)S(1)} %bitcast.90), channel_id=5, replica_groups=mesh['rep'=2,'fs'=32,'tp_0'=4,'tp_1'=2] {'tp_0'}, dimensions={0}, use_global_device_ids=true | all-gather | bytes 983040 | tf_op jit(solution)/shard_map/all_gather | solution.py:26
  46.8 1.9 convert_bitcast_fusion
  48.7 2.4 copy.29
  51.1 1.8 fusion
  52.9 1.1 fusion.95
  54.0 1.3 constant_dynamic-slice_fusion
  55.3 1.5 fusion.8
  56.8 93.8 %all-gather.7.cloned.1.call-done = bf16[2048,768]{1,0:T(8,128)(2,1)} async-done(((bf16[64,768]{1,0:T(8,128)(2,1)}), bf16[2048,768]{1,0:T(8,128)(2,1)}) %all-gather.7.cloned.1.call-update) | async-done | bytes 3145744 | tf_op jit(solution)/shard_map/all_gather | solution.py:57
  150.7 2.3 fusion.23
  153.0 1.8 convolution_multiply_fusion
  154.8 1.6 fusion.93
  157.0 25.9 %all-to-all-start = ((f32[8,1,768]{2,1,0:T(1,128)}), f32[8,1,768]{2,1,0:T(1,128)S(1)}, u32[]{:S(2)}, u32[]{:S(2)}) async-start(f32[8,1,768]{2,1,0:T(1,128)} %broadcast_in_dim.4), calls=%async_computation | async-start | bytes 49152 | tf_op jit(solution)/shard_map/all_to_all | solution.py:62
  183.7 3.9 %all-to-all-done = f32[8,1,768]{2,1,0:T(1,128)S(1)} async-done(((f32[8,1,768]{2,1,0:T(1,128)}), f32[8,1,768]{2,1,0:T(1,128)S(1)}, u32[]{:S(2)}, u32[]{:S(2)}) %all-to-all-start) | async-done | bytes 24608 | tf_op jit(solution)/shard_map/all_to_all | solution.py:62
  187.9 1.8 convolution_convert_fusion
  189.9 23.8 %all_to_all.21 = bf16[8,384,256]{2,1,0:T(8,128)(2,1)S(1)} all-to-all(bf16[8,384,256]{2,1,0:T(8,128)(2,1)S(1)} %bitcast.84), channel_id=1, replica_groups=mesh['rep'=2,'fs'=32,'tp_0'=4,'tp_1'=2] {'tp_0','tp_1'}, dimensions={0} | all-to-all | bytes 3145728 | tf_op jit(solution)/shard_map/all_to_all | solution.py:85
  214.3 24.0 %all_to_all.22 = bf16[8,384,256]{1,2,0:T(8,128)(2,1)S(1)} all-to-all(bf16[8,384,256]{1,2,0:T(8,128)(2,1)S(1)} %broadcast_in_dim.5), channel_id=1, replica_groups=mesh['rep'=2,'fs'=32,'tp_0'=4,'tp_1'=2] {'tp_0','tp_1'}, dimensions={0} | all-to-all | bytes 3145728 | tf_op jit(solution)/shard_map/all_to_all | solution.py:62
  239.2 73.5 %all-gather.9.cloned.1.call-done = bf16[2048,1536]{1,0:T(8,128)(2,1)} async-done(((bf16[64,1536]{1,0:T(8,128)(2,1)}), bf16[2048,1536]{1,0:T(8,128)(2,1)}) %all-gather.9.cloned.1.call-update) | async-done | bytes 6291472 | tf_op jit(solution)/shard_map/all_gather | solution.py:57
  312.7 6.0 %fusion.9 = bf16[384,2048]{1,0:T(8,128)(2,1)S(1)} fusion(bf16[2048,1536]{1,0:T(8,128)(2,1)} %all-gather.9.cloned.1.call-done, bf16[384,2048]{0,1:T(8,128)(2,1)S(1)} %fusion.6), kind=kOutput, calls=%fused_computation.16 | convolution fusion | flops 2417590272 | bytes 9437184 | tf_op jit(solution)/shard_map/dot_general | solution.py:101
  318.8 45.7 %all_to_all.23 = bf16[8,384,256]{2,1,0:T(8,128)(2,1)S(1)} all-to-all(bf16[8,384,256]{2,1,0:T(8,128)(2,1)S(1)} %bitcast.85), channel_id=1, replica_groups=mesh['rep'=2,'fs'=32,'tp_0'=4,'tp_1'=2] {'tp_0','tp_1'}, dimensions={0} | all-to-all | bytes 3145728 | tf_op jit(solution)/shard_map/all_to_all | solution.py:85
  (36 shorter events, 6.2 us)
Async XLA Ops:
  6.5 144.1 %all-gather.7.cloned.1.call-start = ((), (), s32[]{:S(2)}) async-start(), calls=%async_computation.4 | async-start | bytes 3244032 | tf_op jit(solution)/shard_map/all_gather | solution.py:57
  8.0 304.7 %all-gather.9.cloned.1.call-start = ((), (), s32[]{:S(2)}) async-start(), calls=%async_computation.5 | async-start | bytes 6488064 | tf_op jit(solution)/shard_map/all_gather | solution.py:57
  32.1 13.8 %copy-start = (bf16[4,2,192,256]{3,2,1,0:T(8,128)(2,1)}, bf16[4,2,192,256]{3,2,1,0:T(8,128)(2,1)S(1)}, u32[]{:S(2)}) copy-start(bf16[4,2,192,256]{3,2,1,0:T(8,128)(2,1)S(1)} %copy.28) | copy-start | bytes 2359300
  45.9 0.9 copy-start.1
  48.7 6.6 %copy-start.4 = (f32[2048]{0:T(1024)S(1)}, f32[2048]{0:T(1024)}, u32[]{:S(2)}) copy-start(f32[2048]{0:T(1024)} %param.11) | copy-start | bytes 24580
  56.8 96.2 %copy-start.2 = (bf16[384,2048]{0,1:T(8,128)(2,1)S(1)}, bf16[384,2048]{0,1:T(8,128)(2,1)}, u32[]{:S(2)}) copy-start(bf16[384,2048]{0,1:T(8,128)(2,1)} %fusion.8) | copy-start | bytes 4718596
  157.0 30.6 %all-to-all-start = ((f32[8,1,768]{2,1,0:T(1,128)}), f32[8,1,768]{2,1,0:T(1,128)S(1)}, u32[]{:S(2)}, u32[]{:S(2)}) async-start(f32[8,1,768]{2,1,0:T(1,128)} %broadcast_in_dim.4), calls=%async_computation | async-start | bytes 49152 | tf_op jit(solution)/shard_map/all_to_all | solution.py:62
  189.9 24.1 %copy-start.3 = (bf16[384,256]{1,0:T(8,128)(2,1)S(1)}, bf16[384,256]{1,0:T(8,128)(2,1)}, u32[]{:S(2)}) copy-start(bf16[384,256]{1,0:T(8,128)(2,1)} %param.10) | copy-start | bytes 589828
  214.2 24.6 %copy-start.5 = (f32[2048]{0:T(1024)S(1)}, f32[2048]{0:T(1024)}, u32[]{:S(2)}) copy-start(f32[2048]{0:T(1024)} %param.17) | copy-start | bytes 24580
Sparse Core Ops, SparseCore 0:
  9.4 141.2 all-gather.6
  152.8 159.8 all-gather.8
where the time goes:
time: 373 us; the launch traced here: 372 us
  waiting for transfers between devices  171 us (46%)
  blocking collectives  129 us (35%)
  starting transfers between devices  26 us (7%)
  between operations  13.6 us (4%)
  other arithmetic  12.2 us (3%)
  matrix products  12 us (3%)
  local copies, waits for them, and re-layouts  8.6 us (2%)
    all_gather x2, waiting for transfers between devices, in_one_piece(): lax.all_gather(both, axis, axis=dim, tiled=True)  167 us
    all_to_all x2, blocking collectives, summed_on_arrival(): lax.all_to_all(in_blocks(shard, dim, count), axis, 0, 0, tiled=True)  69.5 us
    all_gather x4, blocking collectives, gather_in_order(): pieces = lax.all_gather(pieces, axes[k])  35.1 us
    all_to_all x1, starting transfers between devices, copy_for_each(): return lax.all_to_all(copies, axis, split_axis=0, concat_axis=0, tiled=True)  25.9 us
    all_to_all x1, blocking collectives, copy_for_each(): return lax.all_to_all(copies, axis, split_axis=0, concat_axis=0, tiled=True)  24 us
    dot_general x2, matrix products, times_transposed(): lax.dot_general(left, right, (((1,), (1,)), ((), ())), preferred_element_...  7.85 us
  transfers between devices with their start and end apart: 3, of which 3 were waited for; matrix products, arithmetic and copies ran while one was open for 6% of the time, Pallas kernels for 0%

commit v1 on v0

--- a/solution.py
+++ b/solution.py
@@ -48,13 +48,20 @@
     return laid_out(jnp.concatenate(outs, axis=split_at + 1), dim)
 
 
-def in_one_piece(arrays, axis, dim, along):
-    ends, at = ([], 0)
-    for a in arrays[:-1]:
-        at += a.shape[along]
+def half_of(weight):
+    width = weight.shape[1] // 2
+    return lax.dynamic_slice_in_dim(weight, lax.axis_index("rep") * width, width, 1)
+
+
+def whole_halves(weights):
+    mine = jnp.concatenate([half_of(w) for w in weights], axis=1)
+    pieces = lax.all_gather(mine, ("rep", "fs"), axis=0, tiled=True)
+    pieces = pieces.reshape(2, -1, mine.shape[1])
+    ends, at = [], 0
+    for w in weights[:-1]:
+        at += w.shape[1] // 2
         ends.append(at)
-    both = jnp.concatenate(arrays, axis=along)
-    return tuple(jnp.split(lax.all_gather(both, axis, axis=dim, tiled=True), ends, axis=along))
+    return [jnp.split(pieces[r], ends, axis=1) for r in range(2)]
 
 
 def copy_for_each(shard, axis):
@@ -111,9 +118,13 @@
     token_rows = states.shape[0]
     whole_rows = gather_at_once(states, TP, 1)
     normed = rms_norm(whole_rows, mix_gain)
-    value_full, gate_full, out_full = in_one_piece((w_value, w_gate, w_mix_out), "fs", 0, 1)
-    value = jnp.dot(normed, value_full, preferred_element_type=jnp.float32)
-    gate = jnp.dot(normed, gate_full, preferred_element_type=jnp.float32)
+    mix = whole_halves((w_value, w_gate, w_mix_out))
+    value = jnp.concatenate(
+        [jnp.dot(normed, h[0], preferred_element_type=jnp.float32) for h in mix], axis=1
+    )
+    gate = jnp.concatenate(
+        [jnp.dot(normed, h[1], preferred_element_type=jnp.float32) for h in mix], axis=1
+    )
     gated = value * jax.nn.sigmoid(gate)
     own_kernel = lax.dynamic_slice_in_dim(conv_kernel, offset, width, 1)
     blocks = gated.reshape(token_rows // LENGTH, LENGTH, width)
@@ -131,15 +142,16 @@
     activated = jax.nn.silu((filtered - mean_rows) * lax.rsqrt(variance + EPS) * own_gain).astype(
         jnp.bfloat16
     )
-    mixer_terms = times_transposed(activated, out_full)
+    mixer_terms = times_transposed(activated, jnp.concatenate([h[2] for h in mix], axis=1))
     mixed = summed_on_arrival(mixer_terms.astype(jnp.bfloat16), TP, 1)
     middle = (states.astype(jnp.float32) + mixed).astype(jnp.bfloat16)
     middle_rows = collect(middle, TP, 1)
     normed_mid = rms_norm(middle_rows, mlp_gain)
-    up_full, down_full = in_one_piece((w_up, w_down_t), "fs", 0, 1)
-    upward = jnp.dot(normed_mid, up_full, preferred_element_type=jnp.float32)
-    hidden = jnp.square(jnp.maximum(upward, 0.0)).astype(jnp.bfloat16)
-    fed_terms = times_transposed(hidden, down_full)
+    fed_terms = 0.0
+    for up, down in whole_halves((w_up, w_down_t)):
+        upward = jnp.dot(normed_mid, up, preferred_element_type=jnp.float32)
+        hidden = jnp.square(jnp.maximum(upward, 0.0)).astype(jnp.bfloat16)
+        fed_terms = fed_terms + times_transposed(hidden, down)
     fed = summed_on_arrival(fed_terms.astype(jnp.bfloat16), TP, 1)
     return (middle.astype(jnp.float32) + fed).astype(jnp.bfloat16)
 

time: 373 us -> 236 us (0.63)
  waiting for transfers between devices: 171 us -> 59.6 us
  blocking collectives: 129 us -> 109 us
  starting transfers between devices: 26 us -> 8.62 us
  local copies, waits for them, and re-layouts: 8.6 us -> 14.1 us
  matrix products: 12 us -> 17.2 us
    all_gather x2, waiting for transfers between devices: 167 us -> 56.3 us  [whole_halves(): pieces = lax.all_gather(mine, ('rep', 'fs'), axis=0, tiled=True)]
    all_to_all x2, blocking collectives: 69.5 us -> 50.3 us  [summed_on_arrival(): lax.all_to_all(in_blocks(shard, dim, count), axis, 0, 0, tiled=True)]
    all_to_all x1, starting transfers between devices: 25.9 us -> 8.58 us  [copy_for_each(): return lax.all_to_all(copies, axis, split_axis=0, concat_axis=0, tiled=True)]
    dot_general x2 -> x3, matrix products: 7.85 us -> 10.8 us  [times_transposed(): lax.dot_general(left, right, (((1,), (1,)), ((), ())), preferred_element_...]
  transfers between devices with their start and end apart: 3 -> 3, of which waited for: 3 -> 3; matrix products, arithmetic and copies ran while one was open for 6% -> 13% of each run, Pallas kernels for 0% -> 0%
where the time goes in v1:
time: 236 us; the launch traced here: 235 us
  blocking collectives  109 us (46%)
  waiting for transfers between devices  59.6 us (25%)
  matrix products  17.2 us (7%)
  local copies, waits for them, and re-layouts  14.1 us (6%)
  between operations  13.6 us (6%)
  other arithmetic  12.5 us (5%)
  starting transfers between devices  8.62 us (4%)
    all_gather x2, waiting for transfers between devices, whole_halves(): pieces = lax.all_gather(mine, ('rep', 'fs'), axis=0, tiled=True)  56.3 us
    all_to_all x2, blocking collectives, summed_on_arrival(): lax.all_to_all(in_blocks(shard, dim, count), axis, 0, 0, tiled=True)  50.3 us
    all_gather x4, blocking collectives, gather_in_order(): pieces = lax.all_gather(pieces, axes[k])  34.5 us
    all_to_all x1, blocking collectives, copy_for_each(): return lax.all_to_all(copies, axis, split_axis=0, concat_axis=0, tiled=True)  24.1 us
    dot_general x3, matrix products, times_transposed(): lax.dot_general(left, right, (((1,), (1,)), ((), ())), preferred_element_...  10.8 us
    all_to_all x1, starting transfers between devices, copy_for_each(): return lax.all_to_all(copies, axis, split_axis=0, concat_axis=0, tiled=True)  8.58 us
  transfers between devices with their start and end apart: 3, of which 3 were waited for; matrix products, arithmetic and copies ran while one was open for 13% of the time, Pallas kernels for 0%

profile of v1, /device:TPU:1, one launch (start us, length us, event | category | flops | bytes accessed | tf_op | source)
XLA Modules:
  0.0 234.6 jit_solution(18182806777791911851)
XLA Ops:
  11.2 10.8 %all-gather = bf16[768,256]{1,0:T(8,128)(2,1)S(1)} all-gather(bf16[192,256]{1,0:T(8,128)(2,1)S(1)} %get-tuple-element.41), channel_id=2, replica_groups=mesh['rep'=2,'fs'=32,'tp_0'=4,'tp_1'=2] {'tp_0'}, dimensions={0}, use_global_device_ids=true | all-gather | bytes 491520 | tf_op jit(solution)/shard_map/all_gather | solution.py:26
  22.0 10.5 %all-gather.1 = bf16[8,192,256]{2,1,0:T(8,128)(2,1)S(1)} all-gather(bf16[4,192,256]{2,1,0:T(8,128)(2,1)S(1)} %bitcast.103), channel_id=3, replica_groups=mesh['rep'=2,'fs'=32,'tp_0'=4,'tp_1'=2] {'tp_1'}, dimensions={0}, use_global_device_ids=true | all-gather | bytes 1179648 | tf_op jit(solution)/shard_map/all_gather | solution.py:26
  32.6 2.0 all-gather.2
  34.6 11.2 %all-gather.3 = bf16[8,192,256]{2,1,0:T(8,128)(2,1)S(1)} all-gather(bf16[2,192,256]{2,1,0:T(8,128)(2,1)S(1)} %bitcast.104), channel_id=5, replica_groups=mesh['rep'=2,'fs'=32,'tp_0'=4,'tp_1'=2] {'tp_0'}, dimensions={0}, use_global_device_ids=true | all-gather | bytes 983040 | tf_op jit(solution)/shard_map/all_gather | solution.py:26
  47.0 1.8 copy.53
  48.9 2.3 reshape.149
  51.9 1.8 fusion
  54.7 1.3 constant_dynamic-slice_fusion
  56.1 2.2 multiply_convert_fusion
  58.3 38.9 %all-gather.7.cloned.1.call-done = bf16[4096,384]{1,0:T(8,128)(2,1)} async-done(((bf16[64,384]{1,0:T(8,128)(2,1)}), bf16[4096,384]{1,0:T(8,128)(2,1)}) %all-gather.7.cloned.1.call-update) | async-done | bytes 3145744 | tf_op jit(solution)/shard_map/all_gather | solution.py:58
  97.2 1.6 fusion.35
  98.8 1.6 fusion.36
  100.4 1.6 fusion.38
  102.1 1.6 fusion.37
  103.8 4.5 %fusion.109 = (f32[3,128]{1,0:T(4,128)S(1)}, f32[3,128]{1,0:T(4,128)S(1)}, f32[3,128,256]{1,2,0:T(8,128)S(1)}) fusion(f32[3,128,256]{1,2,0:T(8,128)S(1)} %maximum_multiply_fusion, f32[256]{0:T(256)S(1)} %bitcast.119, f32[256]{0:T(256)S(1)} %bitcast.121, f32[256]{0:T(256)S(1)} %bitcast.122, f32[256]{0:T(256)S(1)} %bitcast.123, f32[256]{0:T(256)S(1)} %bitcast.124, ...), kind=kLoop, calls=%fused_computation.159 | loop fusion | flops 6290688 | bytes 821248 | tf_op jit(solution)/shard_map/reduce_sum | solution.py:137
  109.0 8.6 %all-to-all-start = ((f32[8,1,768]{2,1,0:T(1,128)}), f32[8,1,768]{2,1,0:T(1,128)S(1)}, u32[]{:S(2)}, u32[]{:S(2)}) async-start(f32[8,1,768]{2,1,0:T(1,128)} %broadcast_in_dim.4), calls=%async_computation | async-start | bytes 49152 | tf_op jit(solution)/shard_map/all_to_all | solution.py:69
  117.6 1.3 fusion.111
  119.0 3.3 %all-to-all-done = f32[8,1,768]{2,1,0:T(1,128)S(1)} async-done(((f32[8,1,768]{2,1,0:T(1,128)}), f32[8,1,768]{2,1,0:T(1,128)S(1)}, u32[]{:S(2)}, u32[]{:S(2)}) %all-to-all-start) | async-done | bytes 24608 | tf_op jit(solution)/shard_map/all_to_all | solution.py:69
  123.3 23.8 %all_to_all.21 = bf16[8,384,256]{2,1,0:T(8,128)(2,1)S(1)} all-to-all(bf16[8,384,256]{2,1,0:T(8,128)(2,1)S(1)} %bitcast.98), channel_id=1, replica_groups=mesh['rep'=2,'fs'=32,'tp_0'=4,'tp_1'=2] {'tp_0','tp_1'}, dimensions={0} | all-to-all | bytes 3145728 | tf_op jit(solution)/shard_map/all_to_all | solution.py:92
  147.7 24.1 %all_to_all.22 = bf16[8,384,256]{1,2,0:T(8,128)(2,1)S(1)} all-to-all(bf16[8,384,256]{1,2,0:T(8,128)(2,1)S(1)} %broadcast_in_dim.5), channel_id=1, replica_groups=mesh['rep'=2,'fs'=32,'tp_0'=4,'tp_1'=2] {'tp_0','tp_1'}, dimensions={0} | all-to-all | bytes 3145728 | tf_op jit(solution)/shard_map/all_to_all | solution.py:69
  172.6 17.4 %all-gather.9.cloned.1.call-done = bf16[4096,768]{1,0:T(8,128)(2,1)} async-done(((bf16[64,768]{1,0:T(8,128)(2,1)}), bf16[4096,768]{1,0:T(8,128)(2,1)}) %all-gather.9.cloned.1.call-update) | async-done | bytes 6291472 | tf_op jit(solution)/shard_map/all_gather | solution.py:58
  190.0 5.4 %fusion.6 = f32[384,2048]{1,0:T(8,128)} fusion(bf16[4096,768]{1,0:T(8,128)(2,1)} %all-gather.9.cloned.1.call-done, bf16[384,2048]{0,1:T(8,128)(2,1)S(1)} %fusion.2), kind=kOutput, calls=%fused_computation.47 | convolution fusion | flops 1208401920 | bytes 7864320 | tf_op jit(solution)/shard_map/dot_general | solution.py:108
  195.4 4.7 %add_convert_fusion = bf16[384,2048]{1,0:T(8,128)(2,1)S(1)} fusion(f32[384,2048]{1,0:T(8,128)} %fusion.6, bf16[4096,768]{1,0:T(8,128)(2,1)} %all-gather.9.cloned.1.call-done, bf16[384,2048]{0,1:T(8,128)(2,1)S(1)} %fusion.2), kind=kOutput, calls=%fused_computation.37 | convolution fusion | flops 1209974784 | bytes 9437184 | tf_op jit(solution)/shard_map/dot_general | solution.py:108
  200.3 26.5 %all_to_all.23 = bf16[8,384,256]{2,1,0:T(8,128)(2,1)S(1)} all-to-all(bf16[8,384,256]{2,1,0:T(8,128)(2,1)S(1)} %bitcast.99), channel_id=1, replica_groups=mesh['rep'=2,'fs'=32,'tp_0'=4,'tp_1'=2] {'tp_0','tp_1'}, dimensions={0} | all-to-all | bytes 3145728 | tf_op jit(solution)/shard_map/all_to_all | solution.py:92
  (46 shorter events, 12.1 us)
Async XLA Ops:
  6.5 0.8 copy-start
  6.5 90.6 %all-gather.7.cloned.1.call-start = ((), (), s32[]{:S(2)}) async-start(), calls=%async_computation.4 | async-start | bytes 3194880 | tf_op jit(solution)/shard_map/all_gather | solution.py:58
  8.7 181.3 %all-gather.9.cloned.1.call-start = ((), (), s32[]{:S(2)}) async-start(), calls=%async_computation.5 | async-start | bytes 6389760 | tf_op jit(solution)/shard_map/all_gather | solution.py:58
  32.6 13.2 %copy-start.1 = (bf16[4,2,192,256]{3,2,1,0:T(8,128)(2,1)}, bf16[4,2,192,256]{3,2,1,0:T(8,128)(2,1)S(1)}, u32[]{:S(2)}) copy-start(bf16[4,2,192,256]{3,2,1,0:T(8,128)(2,1)S(1)} %copy.52) | copy-start | bytes 2359300
  45.8 0.9 copy-start.2
  48.9 7.2 %copy-start.4 = (f32[2048]{0:T(1024)S(1)}, f32[2048]{0:T(1024)}, u32[]{:S(2)}) copy-start(f32[2048]{0:T(1024)} %param.11) | copy-start | bytes 24580
  109.0 13.3 %all-to-all-start = ((f32[8,1,768]{2,1,0:T(1,128)}), f32[8,1,768]{2,1,0:T(1,128)S(1)}, u32[]{:S(2)}, u32[]{:S(2)}) async-start(f32[8,1,768]{2,1,0:T(1,128)} %broadcast_in_dim.4), calls=%async_computation | async-start | bytes 49152 | tf_op jit(solution)/shard_map/all_to_all | solution.py:69
  123.3 24.0 %copy-start.3 = (bf16[384,256]{1,0:T(8,128)(2,1)S(1)}, bf16[384,256]{1,0:T(8,128)(2,1)}, u32[]{:S(2)}) copy-start(bf16[384,256]{1,0:T(8,128)(2,1)} %param.10) | copy-start | bytes 589828
  147.7 24.5 %copy-start.5 = (f32[2048]{0:T(1024)S(1)}, f32[2048]{0:T(1024)}, u32[]{:S(2)}) copy-start(f32[2048]{0:T(1024)} %param.17) | copy-start | bytes 24580
Sparse Core Ops, SparseCore 0:
  10.3 86.7 all-gather.6
  100.2 89.7 all-gather.8
